TPU v7x, 32 devices: a whole 2x2x4 slice. The times are simulated.
32 devices in a mesh: grp: 2 (over y), sp: 4 (over z), tp: 4 (over x, core).
Axes of the slice: x: 2, y: 2, z: 4, core: 2. Of those that a mesh axis runs over, the one named last changes fastest.
Arguments:
- hidden_in: bfloat16 [2048, 2048], P(('grp', 'sp')), parts along dimension 0, may hold values from -6 to 6
- query_latent_rows: bfloat16 [2048, 768], P(('grp', 'sp')), parts along dimension 0, may hold values from -6 to 6
- key_value_latent: bfloat16 [2048, 512], P(('grp', 'sp')), parts along dimension 0, may hold values from -6 to 6
- rotary_key: bfloat16 [2048, 32], P(('grp', 'sp')), parts along dimension 0, may hold values from -64 to 64
- query_norm_gain: float32 [768], replicated, may hold values from 0.1 to 1.9
- key_value_gain: float32 [512], replicated, may hold values from 0.1 to 1.9
- query_up_weight: bfloat16 [768, 1536], P(None, 'tp'), may hold values from -0.625 to 0.625
- key_value_up_weight: bfloat16 [512, 2048], P(None, 'tp'), may hold values from -0.25 to 0.25
- out_proj: bfloat16 [1024, 2048], P('tp'), may hold values from -0.1875 to 0.1875
- feed_gain: float32 [2048], replicated, may hold values from 0.1 to 1.9
- feed_up: bfloat16 [2048, 8192], P('sp', 'tp'), may hold values from -0.125 to 0.125
- feed_down: bfloat16 [8192, 2048], P('tp', 'sp'), may hold values from -0.0625 to 0.0625
Outputs:
- layer_out: bfloat16 [2048, 2048], P(('grp', 'sp', 'tp')), parts along dimension 0
There are 2 independent parts, one for each index of `grp`. A program takes and returns all parts, laid end to end along the dimension named above; an argument that names none is the same for every part. Nothing has to cross between parts.
All inputs are finite; a program needn't handle non-finite values.
Results may differ from a plain program's by a relative error of at most 0.02.
Values may be sent and summed in bfloat16 or wider, within the bound.
A program may use at most 128 MiB of HBM per device.

v0:
```python
import math

import jax
import jax.numpy as jnp
from jax import lax
from jax.sharding import PartitionSpec as P

QUERY_KEY_PLAIN = 64
QUERY_KEY_ROTARY = 32
VALUE_HEAD_SIZE = 64


def normalize(values, gain):
    floats = values.astype(jnp.float32)
    return floats * lax.rsqrt(jnp.mean(floats * floats, axis=-1, keepdims=True) + 1e-06) * gain


def rotate(values, position):
    half_size = values.shape[-1] // 2
    inverse = 10000.0 ** (-jnp.arange(half_size, dtype=jnp.float32) * 2.0 / values.shape[-1])
    angles = position[:, None] * inverse[None, :]
    cosine = jnp.concatenate([jnp.cos(angles), jnp.cos(angles)], axis=-1)
    sine = jnp.concatenate([jnp.sin(angles), jnp.sin(angles)], axis=-1)
    shape = (values.shape[0],) + (1,) * (values.ndim - 2) + (values.shape[-1],)
    turned = jnp.concatenate([-values[..., half_size:], values[..., :half_size]], axis=-1)
    return values * cosine.reshape(shape) + turned * sine.reshape(shape)


def on_device(
    hidden_in,
    query_latent_rows,
    key_value_latent,
    rotary_key,
    query_norm_gain,
    key_value_gain,
    query_up_weight,
    key_value_up_weight,
    out_proj,
    feed_gain,
    feed_up,
    feed_down,
):
    tokens_here = hidden_in.shape[0]
    heads_here = query_up_weight.shape[1] // (QUERY_KEY_PLAIN + QUERY_KEY_ROTARY)
    position = (lax.axis_index("sp") * tokens_here + jnp.arange(tokens_here)).astype(jnp.float32)
    scale_factor = (QUERY_KEY_PLAIN + QUERY_KEY_ROTARY) ** (-0.5)
    query_norm = normalize(query_latent_rows, query_norm_gain).astype(jnp.bfloat16)
    queries = jnp.dot(query_norm, query_up_weight, preferred_element_type=jnp.float32).reshape(
        tokens_here, heads_here, QUERY_KEY_PLAIN + QUERY_KEY_ROTARY
    )
    queries = jnp.concatenate(
        [queries[..., :QUERY_KEY_PLAIN], rotate(queries[..., QUERY_KEY_PLAIN:], position)], axis=-1
    ).astype(jnp.bfloat16)
    query_plain = queries[..., :QUERY_KEY_PLAIN]
    query_turned = queries[..., QUERY_KEY_PLAIN:]
    latent = normalize(key_value_latent, key_value_gain).astype(jnp.bfloat16)
    key_rope = rotate(rotary_key.astype(jnp.float32), position).astype(jnp.bfloat16)

    def attend_block(carry, key_plain, value_rows, rope_rows):
        row_max, denom, accum = carry
        scores = jnp.einsum(
            "qhd,khd->hqk", query_plain, key_plain, preferred_element_type=jnp.float32
        )
        scores = scores + jnp.einsum(
            "qhd,kd->hqk", query_turned, rope_rows, preferred_element_type=jnp.float32
        )
        scores = scores * scale_factor
        new_max = jnp.maximum(row_max, jnp.max(scores, axis=-1))
        expo = jnp.exp(scores - new_max[:, :, None])
        factor = jnp.exp(row_max - new_max)
        denom = denom * factor + jnp.sum(expo, axis=-1)
        update = jnp.einsum(
            "hqk,khd->qhd",
            expo.astype(jnp.bfloat16),
            value_rows,
            preferred_element_type=jnp.float32,
        )
        accum = accum * jnp.transpose(factor)[:, :, None] + update
        return (new_max, denom, accum)

    start_carry = (
        jnp.full((heads_here, tokens_here), -1e30, jnp.float32),
        jnp.zeros((heads_here, tokens_here), jnp.float32),
        jnp.zeros((tokens_here, heads_here, VALUE_HEAD_SIZE), jnp.float32),
    )
    own_keys = jnp.dot(latent, key_value_up_weight, preferred_element_type=jnp.float32).astype(
        jnp.bfloat16
    )
    pieces = (
        lax.all_gather(own_keys, "sp", axis=0, tiled=True),
        lax.all_gather(key_rope, "sp", axis=0, tiled=True),
    )
    rows_in = pieces[0].shape[0]
    block = math.gcd(rows_in, 1024)

    def step_block(index, inner):
        first = index * block
        bulk = lax.dynamic_slice_in_dim(pieces[0], first, block, 0)
        rope_rows = lax.dynamic_slice_in_dim(pieces[1], first, block, 0)
        bulk = bulk.reshape(block, heads_here, QUERY_KEY_PLAIN + VALUE_HEAD_SIZE)
        return attend_block(
            inner, bulk[..., :QUERY_KEY_PLAIN], bulk[..., QUERY_KEY_PLAIN:], rope_rows
        )

    final_carry = lax.fori_loop(0, rows_in // block, step_block, start_carry)
    denom = final_carry[1]
    accum = final_carry[2]
    mixed = (
        (accum / jnp.transpose(denom)[:, :, None])
        .astype(jnp.bfloat16)
        .reshape(tokens_here, heads_here * VALUE_HEAD_SIZE)
    )
    share = tokens_here // lax.axis_size("tp")
    lead = lax.axis_index("tp") * share
    branch = lax.psum(
        jnp.dot(mixed, out_proj, preferred_element_type=jnp.float32).astype(jnp.bfloat16), "tp"
    ).astype(jnp.float32)
    middle = (hidden_in.astype(jnp.float32) + branch).astype(jnp.bfloat16)
    normed = normalize(middle, feed_gain).astype(jnp.bfloat16)
    middle_own = lax.dynamic_slice_in_dim(middle, lead, share, 0)
    upward = jnp.dot(
        normed,
        lax.all_gather(feed_up, "sp", axis=0, tiled=True),
        preferred_element_type=jnp.float32,
    )
    activated = jnp.square(jax.nn.relu(upward)).astype(jnp.bfloat16)
    partial_sum = jnp.dot(
        activated,
        lax.all_gather(feed_down, "sp", axis=1, tiled=True),
        preferred_element_type=jnp.float32,
    )
    feed = lax.psum_scatter(
        partial_sum.astype(jnp.bfloat16), "tp", scatter_dimension=0, tiled=True
    ).astype(jnp.float32)
    return (middle_own.astype(jnp.float32) + feed).astype(jnp.bfloat16)


def solution(mesh):
    return jax.shard_map(
        on_device,
        mesh=mesh,
        in_specs=(
            P(("grp", "sp"), None),
            P(("grp", "sp"), None),
            P(("grp", "sp"), None),
            P(("grp", "sp"), None),
            P(),
            P(),
            P(None, "tp"),
            P(None, "tp"),
            P("tp", None),
            P(),
            P("sp", "tp"),
            P("tp", "sp"),
        ),
        out_specs=P(("grp", "sp", "tp"), None),
        check_vma=False,
    )
```

profile of v0, /device:TPU:13, one launch (start us, length us, event | category | flops | bytes accessed | tf_op | source)
XLA Modules:
  0.0 425.5 jit_solution(10657204658215220777)
XLA Ops:
  6.5 1.2 fusion.31
  7.7 2.2 convolution_convert_fusion.2
  10.0 0.7 convert_element_type.75
  10.7 0.7 slice.45
  11.6 0.7 pad_maximum_fusion
  12.3 11.4 %all_gather.13 = bf16[1024,32]{0,1:T(8,128)(2,1)S(1)} all-gather(bf16[256,32]{0,1:T(8,128)(2,1)S(1)} %get-tuple-element.26), channel_id=1, replica_groups=mesh['grp'=2,'sp'=4,'tp'=4] {'sp'}, dimensions={0}, use_global_device_ids=true | all-gather | bytes 81920 | tf_op jit(solution)/shard_map/all_gather | solution.py:91
  23.7 1.2 fusion.26
  24.9 1.7 fusion.37
  26.6 12.5 %all-gather.4.cloned.1.call-done = bf16[1024,512]{1,0:T(8,128)(2,1)} async-done(((bf16[256,512]{1,0:T(8,128)(2,1)}), bf16[1024,512]{1,0:T(8,128)(2,1)}) %all-gather.4.cloned.1.call-update) | async-done | bytes 1048592 | tf_op jit(solution)/shard_map/all_gather | solution.py:90
  39.1 1.5 copy.26
  40.6 0.7 fusion.35
  41.3 0.9 fusion.54
  42.2 1.1 fusion.1
  43.3 0.9 fusion.20
  44.2 1.5 convolution_convert_fusion
  45.7 0.7 all-gather.6.cloned.1.call-update
  46.5 0.5 all-gather.8.cloned.1.call-update
  47.1 34.4 %all-reduce.2.cloned.1.call-done = bf16[256,2048]{1,0:T(8,128)(2,1)} async-done(((bf16[256,2048]{1,0:T(8,128)(2,1)}), bf16[256,2048]{1,0:T(8,128)(2,1)}) %all-reduce.2.cloned.1.call-update) | async-done | bytes 1048592 | tf_op jit(solution)/shard_map/psum | solution.py:115
  81.5 1.7 fusion.5
  83.2 147.6 %all-gather.6.cloned.1.call-done = bf16[2048,2048]{1,0:T(8,128)(2,1)} async-done(((bf16[512,2048]{1,0:T(8,128)(2,1)}), bf16[2048,2048]{1,0:T(8,128)(2,1)}) %all-gather.6.cloned.1.call-update) | async-done | bytes 8388624 | tf_op jit(solution)/shard_map/all_gather | solution.py:123
  230.8 149.3 %all-gather.8.cloned.1.call-done = bf16[2048,2048]{1,0:T(8,128)(2,1)} async-done(((bf16[2048,512]{1,0:T(8,128)(2,1)}), bf16[2048,2048]{1,0:T(8,128)(2,1)}) %all-gather.8.cloned.1.call-update) | async-done | bytes 8388624 | tf_op jit(solution)/shard_map/all_gather | solution.py:129
  380.1 11.3 %convolution_convert_fusion.1 = bf16[256,2048]{1,0:T(8,128)(2,1)} fusion(bf16[2048,2048]{1,0:T(8,128)(2,1)} %all-gather.8.cloned.1.call-done, bf16[2048,2048]{1,0:T(8,128)(2,1)} %all-gather.6.cloned.1.call-done, bf16[256,2048]{1,0:T(8,128)(2,1)S(1)} %get-tuple-element.22, f32[2048]{0:T(1024)S(1)} %copy-done.2, f32[256]{0:T(256)S(1)} %add_rsqrt_fusion), kind=kOutput, calls=%fused_computation.11 | convolution fusion | flops 4299161600 | bytes 18883584 | tf_op jit(solution)/shard_map/dot_general | solution.py:127
  391.4 25.9 %reduce-scatter.2.cloned.1.call-done = bf16[64,2048]{1,0:T(8,128)(2,1)} async-done(((bf16[256,2048]{1,0:T(8,128)(2,1)}), bf16[64,2048]{1,0:T(8,128)(2,1)}) %reduce-scatter.2.cloned.1.call-update) | async-done | bytes 262160 | tf_op jit(solution)/shard_map/reduce_scatter | solution.py:132
  417.3 1.7 add_convert_fusion.1
  (23 shorter events, 0.4 us)
Async XLA Ops:
  6.5 37.6 %copy-start = (bf16[256,2048]{1,0:T(8,128)(2,1)S(1)}, bf16[256,2048]{1,0:T(8,128)(2,1)}, u32[]{:S(2)}) copy-start(bf16[256,2048]{1,0:T(8,128)(2,1)} %param.20) | copy-start | bytes 3145732
  6.5 32.6 %all-gather.4.cloned.1.call-start = ((), (), s32[]{:S(2)}) async-start(), calls=%async_computation.1 | async-start | bytes 1310720 | tf_op jit(solution)/shard_map/all_gather | solution.py:90
  9.9 71.5 %all-reduce.2.cloned.1.call-start = ((), (), s32[]{:S(2)}) async-start(), calls=%async_computation.2 | async-start | bytes 2097152 | tf_op jit(solution)/shard_map/psum | solution.py:115
  44.2 37.3 %copy-start.1 = (bf16[256,2048]{1,0:T(8,128)(2,1)S(1)}, bf16[256,2048]{1,0:T(8,128)(2,1)}, u32[]{:S(2)}) copy-start(bf16[256,2048]{1,0:T(8,128)(2,1)} %param.12) | copy-start | bytes 3145732
  45.7 334.4 %copy-start.2 = (f32[2048]{0:T(1024)S(1)}, f32[2048]{0:T(1024)}, u32[]{:S(2)}) copy-start(f32[2048]{0:T(1024)} %param.21) | copy-start | bytes 24580
  45.7 185.1 %all-gather.6.cloned.1.call-start = ((), (), s32[]{:S(2)}) async-start(), calls=%async_computation.3 | async-start | bytes 10485760 | tf_op jit(solution)/shard_map/all_gather | solution.py:123
  46.4 333.6 %all-gather.8.cloned.1.call-start = ((), (), s32[]{:S(2)}) async-start(), calls=%async_computation.4 | async-start | bytes 10485760 | tf_op jit(solution)/shard_map/all_gather | solution.py:129
  47.0 370.3 %reduce-scatter.2.cloned.1.call-start = ((), (), s32[]{:S(2)}) async-start(), calls=%async_computation.5 | async-start | bytes 1310720 | tf_op jit(solution)/shard_map/reduce_scatter | solution.py:132
Sparse Core Ops, SparseCore 0:
  10.1 29.0 all-gather.3
  45.8 35.5 all-reduce.1
  83.0 147.7 all-gather.5
  232.2 147.7 all-gather.7
  391.5 25.7 reduce-scatter.1
where the time goes:
time: 428 us; the launch traced here: 426 us
  waiting for transfers between devices  371 us (87%)
  matrix products  19.1 us (4%)
  between operations  13.2 us (3%)
  blocking collectives  11.4 us (3%)
  other arithmetic  8.51 us (2%)
    all_gather x1, waiting for transfers between devices, on_device(): lax.all_gather(feed_down, 'sp', axis=1, tiled=True)  149 us
    all_gather x1, waiting for transfers between devices, on_device(): lax.all_gather(feed_up, 'sp', axis=0, tiled=True)  148 us
    psum x1, waiting for transfers between devices, on_device(): lax.psum(jnp.dot(mixed, out_proj, preferred_element_type=jnp.float32).ast...  34.4 us
    reduce_scatter x1, waiting for transfers between devices, on_device(): lax.psum_scatter(partial_sum.astype(jnp.bfloat16), 'tp', scatter_dimensio...  25.9 us
    all_gather x1, waiting for transfers between devices, on_device(): lax.all_gather(own_keys, 'sp', axis=0, tiled=True)  12.5 us
    all_gather x1, blocking collectives, on_device(): lax.all_gather(key_rope, 'sp', axis=0, tiled=True)  11.4 us
    dot_general x1, matrix products, on_device(): jnp.dot(activated, lax.all_gather(feed_down, 'sp', axis=1, tiled=True), p...  11.3 us
  transfers between devices with their start and end apart: 5, of which 5 were waited for; matrix products, arithmetic and copies ran while one was open for 2% of the time, Pallas kernels for 0%

commit v1 on v0

--- a/solution.py
+++ b/solution.py
@@ -110,27 +110,25 @@
         .astype(jnp.bfloat16)
         .reshape(tokens_here, heads_here * VALUE_HEAD_SIZE)
     )
+    up_own = lax.all_to_all(feed_up, "sp", split_axis=1, concat_axis=0, tiled=True)
+    down_own = lax.all_to_all(feed_down, "sp", split_axis=0, concat_axis=1, tiled=True)
     share = tokens_here // lax.axis_size("tp")
     lead = lax.axis_index("tp") * share
-    branch = lax.psum(
-        jnp.dot(mixed, out_proj, preferred_element_type=jnp.float32).astype(jnp.bfloat16), "tp"
+    branch = lax.psum_scatter(
+        jnp.dot(mixed, out_proj, preferred_element_type=jnp.float32).astype(jnp.bfloat16),
+        "tp",
+        scatter_dimension=0,
+        tiled=True,
     ).astype(jnp.float32)
-    middle = (hidden_in.astype(jnp.float32) + branch).astype(jnp.bfloat16)
-    normed = normalize(middle, feed_gain).astype(jnp.bfloat16)
-    middle_own = lax.dynamic_slice_in_dim(middle, lead, share, 0)
-    upward = jnp.dot(
-        normed,
-        lax.all_gather(feed_up, "sp", axis=0, tiled=True),
-        preferred_element_type=jnp.float32,
-    )
+    hidden_own = lax.dynamic_slice_in_dim(hidden_in, lead, share, 0)
+    middle_own = (hidden_own.astype(jnp.float32) + branch).astype(jnp.bfloat16)
+    normed_own = normalize(middle_own, feed_gain).astype(jnp.bfloat16)
+    normed = lax.all_gather(normed_own, ("sp", "tp"), axis=0, tiled=True)
+    upward = jnp.dot(normed, up_own, preferred_element_type=jnp.float32)
     activated = jnp.square(jax.nn.relu(upward)).astype(jnp.bfloat16)
-    partial_sum = jnp.dot(
-        activated,
-        lax.all_gather(feed_down, "sp", axis=1, tiled=True),
-        preferred_element_type=jnp.float32,
-    )
+    partial_sum = jnp.dot(activated, down_own, preferred_element_type=jnp.float32)
     feed = lax.psum_scatter(
-        partial_sum.astype(jnp.bfloat16), "tp", scatter_dimension=0, tiled=True
+        partial_sum.astype(jnp.bfloat16), ("sp", "tp"), scatter_dimension=0, tiled=True
     ).astype(jnp.float32)
     return (middle_own.astype(jnp.float32) + feed).astype(jnp.bfloat16)
 

time: 428 us -> 291 us (0.68)
  waiting for transfers between devices: 371 us -> 209 us
  starting transfers between devices: 0.16 us -> 14.5 us
  local copies, waits for them, and re-layouts: 2.2 us -> 12.7 us
    all_gather x2 -> x1, waiting for transfers between devices: 297 us -> 0.01 us  [on_device(): normed = lax.all_gather(normed_own, ('sp', 'tp'), axis=0, tiled=True)]
    all_to_all x0 -> x2, waiting for transfers between devices: none -> 95.6 us  [the longest x1 55.2 us: on_device(): lax.all_to_all(feed_down, 'sp', split_axis=0, concat_axis=1, tiled=True)]
    reduce_scatter x1 -> x2, waiting for transfers between devices: 25.9 us -> 101 us  [the longest x1 75.9 us: on_device(): lax.psum_scatter(partial_sum.astype(jnp.bfloat16), ('sp', 'tp'), scatter_...]
    psum x1 -> x0, waiting for transfers between devices: 34.4 us -> none  [on_device(): lax.psum(jnp.dot(mixed, out_proj, preferred_element_type=jnp.float32).ast...]
    all_to_all x0 -> x2, starting transfers between devices: none -> 14.4 us  [the longest x1 9.8 us: on_device(): lax.all_to_all(feed_up, 'sp', split_axis=1, concat_axis=0, tiled=True)]
    all_to_all x0 -> x2, local copies, waits for them, and re-layouts: none -> 6.58 us  [the longest x1 4.17 us: on_device(): lax.all_to_all(feed_up, 'sp', split_axis=1, concat_axis=0, tiled=True)]
  transfers between devices with their start and end apart: 5 -> 6, of which waited for: 5 -> 5; matrix products, arithmetic and copies ran while one was open for 2% -> 5% of each run, Pallas kernels for 0% -> 0%
where the time goes in v1:
time: 291 us; the launch traced here: 286 us
  waiting for transfers between devices  209 us (72%)
  matrix products  17.1 us (6%)
  starting transfers between devices  14.5 us (5%)
  between operations  13.2 us (5%)
  local copies, waits for them, and re-layouts  12.7 us (4%)
  blocking collectives  11.4 us (4%)
  other arithmetic  8.82 us (3%)
    reduce_scatter x1, waiting for transfers between devices, on_device(): lax.psum_scatter(partial_sum.astype(jnp.bfloat16), ('sp', 'tp'), scatter_...  75.9 us
    all_to_all x1, waiting for transfers between devices, on_device(): lax.all_to_all(feed_down, 'sp', split_axis=0, concat_axis=1, tiled=True)  55.2 us
    all_to_all x1, waiting for transfers between devices, on_device(): lax.all_to_all(feed_up, 'sp', split_axis=1, concat_axis=0, tiled=True)  40.4 us
    reduce_scatter x1, waiting for transfers between devices, on_device(): lax.psum_scatter(jnp.dot(mixed, out_proj, preferred_element_type=jnp.floa...  24.6 us
    all_gather x1, waiting for transfers between devices, on_device(): lax.all_gather(own_keys, 'sp', axis=0, tiled=True)  12.5 us
    all_gather x1, blocking collectives, on_device(): lax.all_gather(key_rope, 'sp', axis=0, tiled=True)  11.4 us
    all_to_all x1, starting transfers between devices, on_device(): lax.all_to_all(feed_up, 'sp', split_axis=1, concat_axis=0, tiled=True)  9.8 us
    dot_general x1, matrix products, on_device(): jnp.dot(activated, down_own, preferred_element_type=jnp.float32)  9.33 us
  transfers between devices with their start and end apart: 6, of which 5 were waited for; matrix products, arithmetic and copies ran while one was open for 5% of the time, Pallas kernels for 0%

profile of v1, /device:TPU:13, one launch (start us, length us, event | category | flops | bytes accessed | tf_op | source)
XLA Modules:
  0.0 286.4 jit_solution(17183125919812808512)
XLA Ops:
  6.5 1.2 fusion.21
  7.7 2.2 convolution_convert_fusion.2
  12.3 11.4 %all_gather.10 = bf16[1024,32]{0,1:T(8,128)(2,1)S(1)} all-gather(bf16[256,32]{0,1:T(8,128)(2,1)S(1)} %get-tuple-element.26), channel_id=1, replica_groups=mesh['grp'=2,'sp'=4,'tp'=4] {'sp'}, dimensions={0}, use_global_device_ids=true | all-gather | bytes 81920 | tf_op jit(solution)/shard_map/all_gather | solution.py:91
  23.7 1.2 fusion.18
  24.9 1.7 fusion.31
  26.6 12.5 %all-gather.3.cloned.1.call-done = bf16[1024,512]{1,0:T(8,128)(2,1)} async-done(((bf16[256,512]{1,0:T(8,128)(2,1)}), bf16[1024,512]{1,0:T(8,128)(2,1)}) %all-gather.3.cloned.1.call-update) | async-done | bytes 1048592 | tf_op jit(solution)/shard_map/all_gather | solution.py:90
  39.1 1.5 copy.33
  41.3 0.9 fusion.48
  42.2 1.1 fusion.1
  43.3 0.9 fusion.15
  44.2 1.4 convolution_convert_fusion.1
  45.7 24.6 %reduce-scatter.3.cloned.1.call-done = bf16[64,2048]{1,0:T(8,128)(2,1)} async-done(((bf16[256,2048]{1,0:T(8,128)(2,1)}), bf16[64,2048]{1,0:T(8,128)(2,1)}) %reduce-scatter.3.cloned.1.call-update) | async-done | bytes 262160 | tf_op jit(solution)/shard_map/reduce_scatter | solution.py:117
  70.3 1.2 fusion.24
  71.5 0.8 fusion.26
  72.4 4.6 %all-to-all-start.1 = ((bf16[4,512,512]{2,1,0:T(8,128)(2,1)}), bf16[4,512,512]{2,1,0:T(8,128)(2,1)S(1)}, u32[]{:S(2)}, u32[]{:S(2)}) async-start(bf16[4,512,512]{2,1,0:T(8,128)(2,1)} %bitcast.46), calls=%async_computation.2 | async-start | bytes 4194304 | tf_op jit(solution)/shard_map/all_to_all | solution.py:114
  77.0 3.9 %copy.28 = bf16[512,2048]{0,1:T(8,128)(2,1)} copy(bf16[512,2048]{1,0:T(8,128)(2,1)} %param.22) | data formatting | bytes 4194304 | tf_op args[10]
  80.9 55.2 %all-to-all-done.1 = bf16[4,512,512]{2,1,0:T(8,128)(2,1)S(1)} async-done(((bf16[4,512,512]{2,1,0:T(8,128)(2,1)}), bf16[4,512,512]{2,1,0:T(8,128)(2,1)S(1)}, u32[]{:S(2)}, u32[]{:S(2)}) %all-to-all-start.1) | async-done | bytes 2097184 | tf_op jit(solution)/shard_map/all_to_all | solution.py:114
  136.1 9.8 %all-to-all-start = ((bf16[512,4,512]{0,2,1:T(8,128)(2,1)}), bf16[512,4,512]{0,2,1:T(8,128)(2,1)}, u32[]{:S(2)}, u32[]{:S(2)}) async-start(bf16[512,4,512]{0,2,1:T(8,128)(2,1)} %bitcast.40), calls=%async_computation.1 | async-start | bytes 4194304 | tf_op jit(solution)/shard_map/all_to_all | solution.py:113
  145.9 2.4 copy.30
  148.3 40.4 %all-to-all-done = bf16[512,4,512]{0,2,1:T(8,128)(2,1)} async-done(((bf16[512,4,512]{0,2,1:T(8,128)(2,1)}), bf16[512,4,512]{0,2,1:T(8,128)(2,1)}, u32[]{:S(2)}, u32[]{:S(2)}) %all-to-all-start) | async-done | bytes 2097184 | tf_op jit(solution)/shard_map/all_to_all | solution.py:113
  188.7 4.2 %copy.29 = bf16[4,512,512]{2,1,0:T(8,128)(2,1)} copy(bf16[4,512,512]{1,2,0:T(8,128)(2,1)} %bitcast.8) | data formatting | bytes 4194304 | tf_op jit(solution)/shard_map/all_to_all | solution.py:113
  192.9 9.3 %convolution_convert_fusion = bf16[1024,2048]{1,0:T(8,128)(2,1)} fusion(bf16[512,2048]{0,1:T(8,128)(2,1)S(1)} %bitcast.47, bf16[1024,2048]{1,0:T(8,128)(2,1)} %all-gather.5.cloned.1.call-done, bf16[2048,512]{1,0:T(8,128)(2,1)} %bitcast.48), kind=kOutput, calls=%fused_computation.3 | convolution fusion | flops 4298637312 | bytes 12582912 | tf_op jit(solution)/shard_map/dot_general | solution.py:129
  202.2 75.9 %reduce-scatter.5.cloned.1.call-done = bf16[64,2048]{1,0:T(8,128)(2,1)} async-done(((bf16[1024,2048]{1,0:T(8,128)(2,1)}), bf16[64,2048]{1,0:T(8,128)(2,1)}) %reduce-scatter.5.cloned.1.call-update) | async-done | bytes 262160 | tf_op jit(solution)/shard_map/reduce_scatter | solution.py:130
  278.1 1.7 fusion.27
  (28 shorter events, 3.3 us)
Async XLA Ops:
  6.5 37.6 %copy-start = (bf16[256,2048]{1,0:T(8,128)(2,1)S(1)}, bf16[256,2048]{1,0:T(8,128)(2,1)}, u32[]{:S(2)}) copy-start(bf16[256,2048]{1,0:T(8,128)(2,1)} %param.20) | copy-start | bytes 3145732
  6.5 32.6 %all-gather.3.cloned.1.call-start = ((), (), s32[]{:S(2)}) async-start(), calls=%async_computation.4 | async-start | bytes 1310720 | tf_op jit(solution)/shard_map/all_gather | solution.py:90
  9.9 60.4 %reduce-scatter.3.cloned.1.call-start = ((), (), s32[]{:S(2)}) async-start(), calls=%async_computation.5 | async-start | bytes 1310720 | tf_op jit(solution)/shard_map/reduce_scatter | solution.py:117
  43.3 28.3 %copy-start.2 = (f32[2048]{0:T(1024)S(1)}, f32[2048]{0:T(1024)}, u32[]{:S(2)}) copy-start(f32[2048]{0:T(1024)} %param.21) | copy-start | bytes 24580
  45.6 147.3 %all-gather.5.cloned.1.call-start = ((), (), s32[]{:S(2)}) async-start(), calls=%async_computation.6 | async-start | bytes 4456448 | tf_op jit(solution)/shard_map/all_gather | solution.py:126
  72.4 63.7 %all-to-all-start.1 = ((bf16[4,512,512]{2,1,0:T(8,128)(2,1)}), bf16[4,512,512]{2,1,0:T(8,128)(2,1)S(1)}, u32[]{:S(2)}, u32[]{:S(2)}) async-start(bf16[4,512,512]{2,1,0:T(8,128)(2,1)} %bitcast.46), calls=%async_computation.2 | async-start | bytes 4194304 | tf_op jit(solution)/shard_map/all_to_all | solution.py:114
  136.1 52.6 %all-to-all-start = ((bf16[512,4,512]{0,2,1:T(8,128)(2,1)}), bf16[512,4,512]{0,2,1:T(8,128)(2,1)}, u32[]{:S(2)}, u32[]{:S(2)}) async-start(bf16[512,4,512]{0,2,1:T(8,128)(2,1)} %bitcast.40), calls=%async_computation.1 | async-start | bytes 4194304 | tf_op jit(solution)/shard_map/all_to_all | solution.py:113
  145.9 132.3 %reduce-scatter.5.cloned.1.call-start = ((), (), s32[]{:S(2)}) async-start(), calls=%async_computation.7 | async-start | bytes 4456448 | tf_op jit(solution)/shard_map/reduce_scatter | solution.py:130
  148.3 44.6 %copy-start.1 = (bf16[512,4,512]{0,2,1:T(8,128)(2,1)S(1)}, bf16[512,4,512]{0,2,1:T(8,128)(2,1)}, u32[]{:S(2)}) copy-start(bf16[512,4,512]{0,2,1:T(8,128)(2,1)} %copy.30) | copy-start | bytes 6291460
Sparse Core Ops, SparseCore 0:
  10.1 29.0 all-gather.2
  45.7 24.4 reduce-scatter.2
  72.5 78.7 all-gather.4
  202.4 75.7 reduce-scatter.4

commit v2 on v1

--- a/solution.py
+++ b/solution.py
@@ -3,6 +3,8 @@
 import jax
 import jax.numpy as jnp
 from jax import lax
+from jax.experimental import pallas as pl
+from jax.experimental.pallas import tpu as pltpu
 from jax.sharding import PartitionSpec as P
 
 QUERY_KEY_PLAIN = 64
@@ -24,6 +26,289 @@
     shape = (values.shape[0],) + (1,) * (values.ndim - 2) + (values.shape[-1],)
     turned = jnp.concatenate([-values[..., half_size:], values[..., :half_size]], axis=-1)
     return values * cosine.reshape(shape) + turned * sine.reshape(shape)
+
+
+MESH = pl.DeviceIdType.MESH
+
+
+def layer_kernel(
+    n, heads, qp, qr, kvr, hidden, op, gain, up, down, out,
+    kv_all, op_pad, mixed, up_all, down_all, part_d, recv_d, middle, norm_all, act, part,
+    rf1, c2, rf2, c3, rf3, ss, rs, ls,
+):
+    g, me, t = lax.axis_index("grp"), lax.axis_index("sp"), lax.axis_index("tp")
+    c, x = lax.rem(t, 2), t // 2
+    rows = kvr.shape[0]
+    share, width = middle.shape
+    piece_k = up.shape[0]
+    hid = down_all.shape[0]
+    half_k, half_h = piece_k // 2, hid // 2
+    wide = down.shape[1]
+    scale_factor = (QUERY_KEY_PLAIN + QUERY_KEY_ROTARY) ** (-0.5)
+
+    def at_z(k):
+        return lax.rem(me + k, n)
+
+    def from_z(k):
+        return lax.rem(me - k + n, n)
+
+    def at_tp(cc, xx):
+        return {"tp": xx * 2 + cc}
+
+    sib, xpeer, ypeer = at_tp(1 - c, x), at_tp(c, 1 - x), {"grp": 1 - g}
+    barrier = pltpu.get_barrier_semaphore()
+    for k in range(1, n):
+        pl.semaphore_signal(barrier, inc=1, device_id={"sp": at_z(k)}, device_id_type=MESH)
+    for peer in (sib, xpeer, at_tp(1 - c, 1 - x), ypeer):
+        pl.semaphore_signal(barrier, inc=1, device_id=peer, device_id_type=MESH)
+    pl.semaphore_wait(barrier, n + 3)
+
+    names = {}
+    sent = []
+
+    def slot(name):
+        if name not in names:
+            names[name] = len(names)
+        return names[name]
+
+    def send(name, src, dst, dev):
+        i = slot(name)
+        copy = pltpu.make_async_remote_copy(
+            src_ref=src, dst_ref=dst, send_sem=ss.at[i], recv_sem=rs.at[i],
+            device_id=dev, device_id_type=MESH,
+        )
+        copy.start()
+        sent.append(copy)
+
+    def land(name, dst):
+        i = slot(name)
+        pltpu.make_async_remote_copy(
+            src_ref=dst, dst_ref=dst, send_sem=ss.at[i], recv_sem=rs.at[i],
+            device_id=sib, device_id_type=MESH,
+        ).wait_recv()
+
+    def up_half(owner, hv):
+        return up_all.at[pl.ds(pl.multiple_of(owner * piece_k + hv * half_k, half_k), half_k)]
+
+    def down_half(owner, hv):
+        return down_all.at[
+            pl.ds(pl.multiple_of(hv * half_h, half_h), half_h),
+            pl.ds(pl.multiple_of(owner * wide, wide), wide),
+        ]
+
+    for k in range(1, n):
+        send(("kv", k), kvr, kv_all.at[me], {"sp": at_z(k)})
+    for k in range(1, n):
+        send(
+            ("up", k),
+            up.at[
+                pl.ds(pl.multiple_of(g * half_k, half_k), half_k),
+                pl.ds(pl.multiple_of(at_z(k) * hid, hid), hid),
+            ],
+            up_half(me, g),
+            {"sp": at_z(k)},
+        )
+    local = [
+        pltpu.make_async_copy(
+            up.at[:, pl.ds(pl.multiple_of(me * hid, hid), hid)],
+            up_all.at[pl.ds(pl.multiple_of(me * piece_k, piece_k), piece_k)],
+            ls.at[0],
+        ),
+        pltpu.make_async_copy(
+            down.at[pl.ds(pl.multiple_of(me * hid, hid), hid)],
+            down_all.at[:, pl.ds(pl.multiple_of(me * wide, wide), wide)],
+            ls.at[1],
+        ),
+    ]
+    for copy in local:
+        copy.start()
+    kv_all[me] = kvr[...]
+    vh = VALUE_HEAD_SIZE
+    unit = QUERY_KEY_PLAIN + vh
+    for h in range(heads):
+        op_pad[h * unit : h * unit + QUERY_KEY_PLAIN] = jnp.zeros((QUERY_KEY_PLAIN, width), op.dtype)
+        op_pad[h * unit + QUERY_KEY_PLAIN : (h + 1) * unit] = op[h * vh : (h + 1) * vh]
+    for k in range(1, n):
+        land(("kv", k), kv_all.at[from_z(k)])
+
+    contract = (((1,), (1,)), ((), ()))
+    rope = kv_all[:, :, heads * unit :].reshape(n * rows, -1)
+    for h in range(heads):
+        kv = kv_all[:, :, h * unit : (h + 1) * unit].reshape(n * rows, unit)
+        scores = lax.dot_general(qp[h], kv, contract, preferred_element_type=jnp.float32)
+        scores += lax.dot_general(qr[h], rope, contract, preferred_element_type=jnp.float32)
+        scores = scores * scale_factor
+        expo = jnp.exp(scores - jnp.max(scores, axis=-1, keepdims=True))
+        total = jnp.sum(expo, axis=-1, keepdims=True)
+        mix = jnp.dot(expo.astype(jnp.bfloat16), kv, preferred_element_type=jnp.float32)
+        mixed[:, h * unit : (h + 1) * unit] = (mix / total).astype(jnp.bfloat16)
+
+    tile = math.gcd(width, 512)
+
+    @pl.loop(0, width // tile)
+    def _(j):
+        cols = pl.ds(pl.multiple_of(j * tile, tile), tile)
+        part_d[:, cols] = jnp.dot(
+            mixed[...], op_pad[:, cols], preferred_element_type=jnp.float32
+        ).astype(jnp.bfloat16)
+
+    def own_rows(cc, xx):
+        return pl.ds(pl.multiple_of((xx * 2 + cc) * share, share), share)
+
+    others = ((c, 1 - x), (1 - c, 1 - x), (1 - c, x))
+    for j, (cc, xx) in enumerate(others):
+        send(("d", j), part_d.at[own_rows(cc, xx)], recv_d.at[j], at_tp(cc, xx))
+    branch = part_d[own_rows(c, x)].astype(jnp.float32)
+    for j in range(3):
+        land(("d", j), recv_d.at[j])
+        branch += recv_d[j].astype(jnp.float32)
+    middle[...] = (hidden[own_rows(c, x)].astype(jnp.float32) + branch).astype(jnp.bfloat16)
+    norm_all[me, c, x] = normalize(middle[...], gain[...]).astype(jnp.bfloat16)
+
+    own = norm_all.at[me, c, x]
+    for k in range(1, n):
+        send(("nz", k), own, own, {"sp": at_z(k)})
+    send(("nx", 0), own, own, xpeer)
+    send(("ns", 0), own, own, sib)
+    for k in range(1, n):
+        send(
+            ("dn", k),
+            down.at[pl.ds(pl.multiple_of(at_z(k) * hid + g * half_h, half_h), half_h)],
+            down_half(me, g),
+            {"sp": at_z(k)},
+        )
+    for k in range(1, n):
+        piece = up_half(from_z(k), g)
+        land(("up", k), piece)
+        send(("uy", k), piece, piece, ypeer)
+    for k in range(1, n):
+        piece = norm_all.at[from_z(k), c, x]
+        land(("nz", k), piece)
+        send(("nx", k), piece, piece, xpeer)
+        send(("ns", k), piece, piece, sib)
+    for k in range(n):
+        piece = norm_all.at[from_z(k), c, 1 - x]
+        land(("nx", k), piece)
+        send(("nt", k), piece, piece, sib)
+    for k in range(1, n):
+        land(("uy", k), up_half(from_z(k), 1 - g))
+    local[0].wait()
+    for k in range(n):
+        land(("ns", k), norm_all.at[from_z(k), 1 - c, x])
+        land(("nt", k), norm_all.at[from_z(k), 1 - c, 1 - x])
+
+    @pl.loop(0, n)
+    def _(j):
+        upward = jnp.dot(
+            norm_all[j].reshape(rows, width), up_all[...], preferred_element_type=jnp.float32
+        )
+        act[j] = jnp.square(jnp.maximum(upward, 0.0)).astype(jnp.bfloat16)
+
+    for k in range(1, n):
+        piece = down_half(from_z(k), g)
+        land(("dn", k), piece)
+        send(("dy", k), piece, piece, ypeer)
+    for k in range(1, n):
+        land(("dy", k), down_half(from_z(k), 1 - g))
+    local[1].wait()
+
+    order = [*range(1, n), 0]
+    for k in order:
+        dest = at_z(k)
+
+        @pl.loop(0, width // tile)
+        def _(j):
+            cols = pl.ds(pl.multiple_of(j * tile, tile), tile)
+            made = jnp.dot(act[dest], down_all[:, cols], preferred_element_type=jnp.float32)
+            part[k, :, :, :, cols] = made.astype(jnp.bfloat16).reshape(2, 2, share, tile)
+
+        send(("f1", k), part.at[k, 1 - c], rf1.at[k], sib)
+    for k in order:
+        land(("f1", k), rf1.at[k])
+        c2[k] = (
+            part[k, c, 1 - x].astype(jnp.float32) + rf1[k, 1 - x].astype(jnp.float32)
+        ).astype(jnp.bfloat16)
+        send(("f2", k), c2.at[k], rf2.at[k], xpeer)
+    for k in order:
+        land(("f2", k), rf2.at[k])
+        c3[k] = (
+            part[k, c, x].astype(jnp.float32)
+            + rf1[k, x].astype(jnp.float32)
+            + rf2[k].astype(jnp.float32)
+        ).astype(jnp.bfloat16)
+        if k:
+            send(("f3", k), c3.at[k], rf3.at[k], {"sp": at_z(k)})
+    feed = c3[0].astype(jnp.float32)
+    for k in range(1, n):
+        land(("f3", k), rf3.at[k])
+        feed += rf3[k].astype(jnp.float32)
+    out[...] = (middle[...].astype(jnp.float32) + feed).astype(jnp.bfloat16)
+    for copy in sent:
+        copy.wait_send()
+
+
+def run_layer(queries, own_keys, key_rope, hidden_in, out_proj, feed_gain, feed_up, feed_down):
+    n = lax.axis_size("sp")
+    rows, heads, size = queries.shape
+    width = hidden_in.shape[1]
+    share = rows // lax.axis_size("tp")
+    hid = feed_up.shape[1] // n
+    turned = jnp.transpose(queries, (1, 0, 2))
+    unit = QUERY_KEY_PLAIN + VALUE_HEAD_SIZE
+    plain = jnp.pad(turned[..., :QUERY_KEY_PLAIN], ((0, 0), (0, 0), (0, VALUE_HEAD_SIZE)))
+    rotary = jnp.pad(turned[..., QUERY_KEY_PLAIN:], ((0, 0), (0, 0), (0, unit - QUERY_KEY_ROTARY)))
+    kvr = jnp.concatenate(
+        [own_keys, jnp.pad(key_rope, ((0, 0), (0, unit - QUERY_KEY_ROTARY)))], axis=1
+    )
+    bf = jnp.bfloat16
+    vmem = pl.BlockSpec(memory_space=pltpu.VMEM)
+    anywhere = pl.BlockSpec(memory_space=pl.ANY)
+    copies = 12 * n
+    block = (share, width)
+    return pl.pallas_call(
+        lambda *refs: layer_kernel(n, heads, *refs),
+        out_shape=jax.ShapeDtypeStruct(block, bf),
+        in_specs=[vmem] * 6 + [anywhere] * 2,
+        out_specs=vmem,
+        scratch_shapes=[
+            pltpu.VMEM((n, *kvr.shape), bf),
+            pltpu.VMEM((heads * unit, width), bf),
+            pltpu.VMEM((rows, heads * unit), bf),
+            pltpu.VMEM((feed_up.shape[0] * n, hid), bf),
+            pltpu.VMEM((hid, feed_down.shape[1] * n), bf),
+            pltpu.VMEM((rows, width), bf),
+            pltpu.VMEM((3, *block), bf),
+            pltpu.VMEM(block, bf),
+            pltpu.VMEM((n, 2, 2, *block), bf),
+            pltpu.VMEM((n, rows, hid), bf),
+            pltpu.VMEM((n, 2, 2, *block), bf),
+            pltpu.VMEM((n, 2, *block), bf),
+            pltpu.VMEM((n, *block), bf),
+            pltpu.VMEM((n, *block), bf),
+            pltpu.VMEM((n, *block), bf),
+            pltpu.VMEM((n, *block), bf),
+            pltpu.SemaphoreType.DMA((copies,)),
+            pltpu.SemaphoreType.DMA((copies,)),
+            pltpu.SemaphoreType.DMA((2,)),
+        ],
+        compiler_params=pltpu.CompilerParams(
+            collective_id=0, has_side_effects=True, vmem_limit_bytes=60 * 1024 * 1024
+        ),
+    )(plain, rotary, kvr, hidden_in, out_proj, feed_gain.reshape(1, -1), feed_up, feed_down)
+
+
+def fits_kernel(tokens, feed_up):
+    n = lax.axis_size("sp")
+    hid = feed_up.shape[1] // n
+    return (
+        lax.axis_size("grp") == 2
+        and lax.axis_size("tp") == 4
+        and 1 < n
+        and tokens * n <= 1024
+        and tokens % 64 == 0
+        and hid % 128 == 0
+        and hid <= 512
+    )
 
 
 def on_device(
@@ -86,6 +371,10 @@
     own_keys = jnp.dot(latent, key_value_up_weight, preferred_element_type=jnp.float32).astype(
         jnp.bfloat16
     )
+    if fits_kernel(tokens_here, feed_up):
+        return run_layer(
+            queries, own_keys, key_rope, hidden_in, out_proj, feed_gain, feed_up, feed_down
+        )
     pieces = (
         lax.all_gather(own_keys, "sp", axis=0, tiled=True),
         lax.all_gather(key_rope, "sp", axis=0, tiled=True),

time: 291 us -> 174 us (0.60); the launches traced: 286 us -> 173 us
  waiting for transfers between devices: 209 us -> 0 us
  Pallas kernels: 0 us -> 164 us
  matrix products: 17.1 us -> 1.78 us
  starting transfers between devices: 14.5 us -> 0 us
  between operations: 13.2 us -> 0.23 us
  blocking collectives: 11.4 us -> 0 us
  local copies, waits for them, and re-layouts: 12.7 us -> 4.43 us
  other arithmetic: 8.82 us -> 2.64 us
    pallas_call x0 -> x1, Pallas kernels: none -> 164 us  [run_layer(): pl.pallas_call(lambda *refs: layer_kernel(n, heads, *refs), out_shape=jax...]
    reduce_scatter x2 -> x0, waiting for transfers between devices: 101 us -> none  [the longest x1 75.9 us: on_device(): lax.psum_scatter(partial_sum.astype(jnp.bfloat16), ('sp', 'tp'), scatter_...]
    all_to_all x2 -> x0, waiting for transfers between devices: 95.6 us -> none  [the longest x1 55.2 us: on_device(): lax.all_to_all(feed_down, 'sp', split_axis=0, concat_axis=1, tiled=True)]
    all_to_all x2 -> x0, starting transfers between devices: 14.4 us -> none  [the longest x1 9.8 us: on_device(): lax.all_to_all(feed_up, 'sp', split_axis=1, concat_axis=0, tiled=True)]
    dot_general x5 -> x0, matrix products: 13.2 us -> none  [the longest x1 9.33 us: on_device(): jnp.dot(activated, down_own, preferred_element_type=jnp.float32)]
    all_gather x2 -> x0, waiting for transfers between devices: 12.5 us -> none  [the longest x1 12.5 us: on_device(): lax.all_gather(own_keys, 'sp', axis=0, tiled=True)]
    all_gather x1 -> x0, blocking collectives: 11.4 us -> none  [on_device(): lax.all_gather(key_rope, 'sp', axis=0, tiled=True)]
    all_to_all x2 -> x0, local copies, waits for them, and re-layouts: 6.58 us -> none  [the longest x1 4.17 us: on_device(): lax.all_to_all(feed_up, 'sp', split_axis=1, concat_axis=0, tiled=True)]
  transfers between devices with their start and end apart: 6 -> 0, of which waited for: 5 -> 0; matrix products, arithmetic and copies ran while one was open for 5% -> 0% of each run, Pallas kernels for 0% -> 0%
where the time goes in v2:
time: 174 us; the launch traced here: 173 us
  Pallas kernels  164 us (94%)
  local copies, waits for them, and re-layouts  4.43 us (3%)
  other arithmetic  2.64 us (2%)
  matrix products  1.78 us (1%)
    pallas_call x1, Pallas kernels, run_layer(): pl.pallas_call(lambda *refs: layer_kernel(n, heads, *refs), out_shape=jax...  164 us

profile of v2, /device:TPU:13, one launch (start us, length us, event | category | flops | bytes accessed | tf_op | source)
XLA Modules:
  0.0 172.6 jit_solution(3688522031899303862)
XLA Ops:
  0.0 1.2 fusion
  1.2 1.4 fusion.7
  2.7 0.2 copy.46
  3.0 0.1 multiply_cosine_fusion
  3.1 0.1 copy.44
  3.2 0.1 copy.45
  3.3 0.2 copy.54
  3.5 0.1 add_convert_fusion
  3.7 0.0 copy-start.1
  3.7 0.2 copy.53
  3.9 0.0 copy-start.4
  3.9 0.1 maximum_bitcast_fusion
  4.0 0.1 slice.40
  4.2 0.8 pad.13.refs_1_
  4.9 0.8 pad.12.refs_0_
  5.7 0.1 copy.49
  5.8 0.1 copy.50
  5.9 0.1 copy.47
  6.0 0.1 fusion.16
  6.1 0.1 fusion.4
  6.3 0.3 convolution_convert_fusion
  6.6 0.7 fusion.11.refs_2_
  7.4 163.5 %shard_map.118 = bf16[64,2048]{1,0:T(8,128)(2,1)} custom-call(bf16[4,256,128]{2,1,0:T(8,128)(2,1)} %pad.12.refs_0_, bf16[4,256,128]{2,1,0:T(8,128)(2,1)} %pad.13.refs_1_, bf16[256,640]{1,0:T(8,128)(2,1)} %fusion.11.refs_2_, bf16[256,2048]{1,0:T(8,128)(2,1)} %refs_3_.1, bf16[256,2048]{1,0:T(8,128)(2,1)} %refs_4_.1, f32[1,2048]{1,0:T(1,128)} %bitcast.11, ...), custom_call_target="tpu_custom_call" | custom-call | tf_op jit(solution)/shard_map/pallas_call | solution.py:268
  170.9 1.7 copy.56
  (19 shorter events, 0.1 us)
Async XLA Ops:
  0.0 1.2 copy-start
  3.5 2.1 %copy-start.2 = (bf16[256,32]{0,1:T(8,128)(2,1)S(1)}, bf16[256,32]{0,1:T(8,128)(2,1)}, u32[]{:S(2)}) copy-start(bf16[256,32]{0,1:T(8,128)(2,1)} %param.15) | copy-start | bytes 49156
  3.7 2.5 %copy-start.1 = (bf16[256,512]{1,0:T(8,128)(2,1)S(1)}, bf16[256,512]{1,0:T(8,128)(2,1)}, u32[]{:S(2)}) copy-start(bf16[256,512]{1,0:T(8,128)(2,1)} %param.14) | copy-start | bytes 786436
  3.8 2.4 %copy-start.3 = (bf16[512,512]{1,0:T(8,128)(2,1)S(1)}, bf16[512,512]{1,0:T(8,128)(2,1)}, u32[]{:S(2)}) copy-start(bf16[512,512]{1,0:T(8,128)(2,1)} %param.19) | copy-start | bytes 1572868
  3.9 2.4 %copy-start.4 = (f32[512]{0:T(512)S(1)}, f32[512]{0:T(512)}, u32[]{:S(2)}) copy-start(f32[512]{0:T(512)} %param.17) | copy-start | bytes 6148

commit v3 on v2

--- a/solution.py
+++ b/solution.py
@@ -32,14 +32,15 @@
 
 
 def layer_kernel(
-    n, heads, qp, qr, kvr, hidden, op, gain, up, down, out,
-    kv_all, op_pad, mixed, up_all, down_all, part_d, recv_d, middle, norm_all, act, part,
+    n, heads, qp, qr, lat, wkv, hidden, op, gain, up, down, out,
+    lat_all, kv_all, op_pad, mixed, up_all, down_all, part_d, recv_d, middle, norm_all, act, part,
     rf1, c2, rf2, c3, rf3, ss, rs, ls,
 ):
     g, me, t = lax.axis_index("grp"), lax.axis_index("sp"), lax.axis_index("tp")
     c, x = lax.rem(t, 2), t // 2
-    rows = kvr.shape[0]
     share, width = middle.shape
+    rows = share * 4
+    rank = wkv.shape[0]
     piece_k = up.shape[0]
     hid = down_all.shape[0]
     half_k, half_h = piece_k // 2, hid // 2
@@ -96,8 +97,37 @@
             pl.ds(pl.multiple_of(owner * wide, wide), wide),
         ]
 
-    for k in range(1, n):
-        send(("kv", k), kvr, kv_all.at[me], {"sp": at_z(k)})
+    def begin(tag, buf):
+        own = buf.at[me, c, x]
+        for k in range(1, n):
+            send((tag, "z", k), own, own, {"sp": at_z(k)})
+        send((tag, "x", 0), own, own, xpeer)
+        send((tag, "s", 0), own, own, sib)
+
+    def finish(tag, buf):
+        for k in range(1, n):
+            piece = buf.at[from_z(k), c, x]
+            land((tag, "z", k), piece)
+            send((tag, "x", k), piece, piece, xpeer)
+            send((tag, "s", k), piece, piece, sib)
+        for k in range(n):
+            piece = buf.at[from_z(k), c, 1 - x]
+            land((tag, "x", k), piece)
+            send((tag, "t", k), piece, piece, sib)
+        for k in range(n):
+            land((tag, "s", k), buf.at[from_z(k), 1 - c, x])
+            land((tag, "t", k), buf.at[from_z(k), 1 - c, 1 - x])
+
+    def send_down(k):
+        send(
+            ("dn", k),
+            down.at[pl.ds(pl.multiple_of(at_z(k) * hid + g * half_h, half_h), half_h)],
+            down_half(me, g),
+            {"sp": at_z(k)},
+        )
+
+    lat_all[me, c, x] = lat[...]
+    begin("l", lat_all)
     for k in range(1, n):
         send(
             ("up", k),
@@ -108,6 +138,7 @@
             up_half(me, g),
             {"sp": at_z(k)},
         )
+    send_down(1)
     local = [
         pltpu.make_async_copy(
             up.at[:, pl.ds(pl.multiple_of(me * hid, hid), hid)],
@@ -122,17 +153,21 @@
     ]
     for copy in local:
         copy.start()
-    kv_all[me] = kvr[...]
     vh = VALUE_HEAD_SIZE
     unit = QUERY_KEY_PLAIN + vh
     for h in range(heads):
         op_pad[h * unit : h * unit + QUERY_KEY_PLAIN] = jnp.zeros((QUERY_KEY_PLAIN, width), op.dtype)
         op_pad[h * unit + QUERY_KEY_PLAIN : (h + 1) * unit] = op[h * vh : (h + 1) * vh]
-    for k in range(1, n):
-        land(("kv", k), kv_all.at[from_z(k)])
+    finish("l", lat_all)
+    for j in range(n):
+        kv_all[j] = jnp.dot(
+            lat_all[j, :, :, :, :rank].reshape(rows, rank),
+            wkv[...],
+            preferred_element_type=jnp.float32,
+        ).astype(jnp.bfloat16)
 
     contract = (((1,), (1,)), ((), ()))
-    rope = kv_all[:, :, heads * unit :].reshape(n * rows, -1)
+    rope = lat_all[:, :, :, :, rank:].reshape(n * rows, -1)
     for h in range(heads):
         kv = kv_all[:, :, h * unit : (h + 1) * unit].reshape(n * rows, unit)
         scores = lax.dot_general(qp[h], kv, contract, preferred_element_type=jnp.float32)
@@ -165,38 +200,17 @@
     middle[...] = (hidden[own_rows(c, x)].astype(jnp.float32) + branch).astype(jnp.bfloat16)
     norm_all[me, c, x] = normalize(middle[...], gain[...]).astype(jnp.bfloat16)
 
-    own = norm_all.at[me, c, x]
-    for k in range(1, n):
-        send(("nz", k), own, own, {"sp": at_z(k)})
-    send(("nx", 0), own, own, xpeer)
-    send(("ns", 0), own, own, sib)
-    for k in range(1, n):
-        send(
-            ("dn", k),
-            down.at[pl.ds(pl.multiple_of(at_z(k) * hid + g * half_h, half_h), half_h)],
-            down_half(me, g),
-            {"sp": at_z(k)},
-        )
+    begin("n", norm_all)
+    for k in range(2, n):
+        send_down(k)
     for k in range(1, n):
         piece = up_half(from_z(k), g)
         land(("up", k), piece)
         send(("uy", k), piece, piece, ypeer)
-    for k in range(1, n):
-        piece = norm_all.at[from_z(k), c, x]
-        land(("nz", k), piece)
-        send(("nx", k), piece, piece, xpeer)
-        send(("ns", k), piece, piece, sib)
-    for k in range(n):
-        piece = norm_all.at[from_z(k), c, 1 - x]
-        land(("nx", k), piece)
-        send(("nt", k), piece, piece, sib)
+    finish("n", norm_all)
     for k in range(1, n):
         land(("uy", k), up_half(from_z(k), 1 - g))
     local[0].wait()
-    for k in range(n):
-        land(("ns", k), norm_all.at[from_z(k), 1 - c, x])
-        land(("nt", k), norm_all.at[from_z(k), 1 - c, 1 - x])
-
     @pl.loop(0, n)
     def _(j):
         upward = jnp.dot(
@@ -247,7 +261,9 @@
         copy.wait_send()
 
 
-def run_layer(queries, own_keys, key_rope, hidden_in, out_proj, feed_gain, feed_up, feed_down):
+def run_layer(
+    queries, latent, key_rope, key_value_up_weight, hidden_in, out_proj, feed_gain, feed_up, feed_down
+):
     n = lax.axis_size("sp")
     rows, heads, size = queries.shape
     width = hidden_in.shape[1]
@@ -257,21 +273,23 @@
     unit = QUERY_KEY_PLAIN + VALUE_HEAD_SIZE
     plain = jnp.pad(turned[..., :QUERY_KEY_PLAIN], ((0, 0), (0, 0), (0, VALUE_HEAD_SIZE)))
     rotary = jnp.pad(turned[..., QUERY_KEY_PLAIN:], ((0, 0), (0, 0), (0, unit - QUERY_KEY_ROTARY)))
-    kvr = jnp.concatenate(
-        [own_keys, jnp.pad(key_rope, ((0, 0), (0, unit - QUERY_KEY_ROTARY)))], axis=1
-    )
+    lat = jnp.concatenate(
+        [latent, jnp.pad(key_rope, ((0, 0), (0, unit - QUERY_KEY_ROTARY)))], axis=1
+    )
+    lat = lax.dynamic_slice_in_dim(lat, lax.axis_index("tp") * share, share, 0)
     bf = jnp.bfloat16
     vmem = pl.BlockSpec(memory_space=pltpu.VMEM)
     anywhere = pl.BlockSpec(memory_space=pl.ANY)
-    copies = 12 * n
+    copies = 16 * n
     block = (share, width)
     return pl.pallas_call(
         lambda *refs: layer_kernel(n, heads, *refs),
         out_shape=jax.ShapeDtypeStruct(block, bf),
-        in_specs=[vmem] * 6 + [anywhere] * 2,
+        in_specs=[vmem] * 7 + [anywhere] * 2,
         out_specs=vmem,
         scratch_shapes=[
-            pltpu.VMEM((n, *kvr.shape), bf),
+            pltpu.VMEM((n, 2, 2, *lat.shape), bf),
+            pltpu.VMEM((n, rows, heads * unit), bf),
             pltpu.VMEM((heads * unit, width), bf),
             pltpu.VMEM((rows, heads * unit), bf),
             pltpu.VMEM((feed_up.shape[0] * n, hid), bf),
@@ -294,7 +312,10 @@
         compiler_params=pltpu.CompilerParams(
             collective_id=0, has_side_effects=True, vmem_limit_bytes=60 * 1024 * 1024
         ),
-    )(plain, rotary, kvr, hidden_in, out_proj, feed_gain.reshape(1, -1), feed_up, feed_down)
+    )(
+        plain, rotary, lat, key_value_up_weight, hidden_in, out_proj,
+        feed_gain.reshape(1, -1), feed_up, feed_down,
+    )
 
 
 def fits_kernel(tokens, feed_up):
@@ -373,7 +394,8 @@
     )
     if fits_kernel(tokens_here, feed_up):
         return run_layer(
-            queries, own_keys, key_rope, hidden_in, out_proj, feed_gain, feed_up, feed_down
+            queries, latent, key_rope, key_value_up_weight, hidden_in, out_proj,
+            feed_gain, feed_up, feed_down,
         )
     pieces = (
         lax.all_gather(own_keys, "sp", axis=0, tiled=True),

time: 174 us -> 166 us (0.954)
  Pallas kernels: 164 us -> 156 us
    pallas_call x1, Pallas kernels: 164 us -> 156 us  [run_layer(): pl.pallas_call(lambda *refs: layer_kernel(n, heads, *refs), out_shape=jax...]
where the time goes in v3:
time: 166 us
  Pallas kernels  156 us (94%)
  local copies, waits for them, and re-layouts  5.85 us (4%)
  other arithmetic  3.65 us (2%)
    pallas_call x1, Pallas kernels, run_layer(): pl.pallas_call(lambda *refs: layer_kernel(n, heads, *refs), out_shape=jax...  156 us

profile of v3, /device:TPU:13, one launch (start us, length us, event | category | flops | bytes accessed | tf_op | source)
XLA Modules:
  0.0 165.7 jit_solution(2776795461504457754)
XLA Ops:
  0.0 0.0 copy-start
  0.1 1.2 fusion
  1.3 1.1 fusion.3
  2.4 0.1 multiply_cosine_fusion
  2.6 0.7 fusion.14
  3.3 0.1 copy.44
  3.4 0.1 copy.49
  3.5 0.1 copy.45
  3.6 0.1 copy.50
  3.7 0.8 copy.47
  4.5 0.1 fusion.12
  4.7 0.1 fusion.5
  4.8 0.7 fusion.13.refs_2_
  5.5 0.4 fusion.6
  6.0 0.2 copy.53
  6.2 0.2 copy.46
  6.4 0.2 copy.54
  6.6 0.1 add_convert_fusion
  6.7 0.1 maximum_bitcast_fusion
  6.8 0.8 pad.12.refs_0_
  7.6 0.1 slice.40
  7.7 0.7 pad.13.refs_1_
  8.5 155.5 %shard_map.118 = bf16[64,2048]{1,0:T(8,128)(2,1)} custom-call(bf16[4,256,128]{2,1,0:T(8,128)(2,1)} %pad.12.refs_0_, bf16[4,256,128]{2,1,0:T(8,128)(2,1)} %pad.13.refs_1_, bf16[64,640]{1,0:T(8,128)(2,1)} %fusion.13.refs_2_, bf16[512,512]{1,0:T(8,128)(2,1)} %refs_3_.1, bf16[256,2048]{1,0:T(8,128)(2,1)} %refs_4_.1, bf16[256,2048]{1,0:T(8,128)(2,1)} %refs_5_.1, ...), custom_call_target="tpu_custom_call" | custom-call | tf_op jit(solution)/shard_map/pallas_call | solution.py:285
  164.0 1.7 %copy.56 = bf16[64,2048]{1,0:T(8,128)(2,1)} copy(bf16[64,2048]{1,0:T(8,128)(2,1)} %shard_map.118) | data formatting | bytes 524288
  (19 shorter events, 0.1 us)
Async XLA Ops:
  0.0 5.5 %copy-start = (bf16[768,384]{1,0:T(8,128)(2,1)S(1)}, bf16[768,384]{1,0:T(8,128)(2,1)}, u32[]{:S(2)}) copy-start(bf16[768,384]{1,0:T(8,128)(2,1)} %param.18) | copy-start | bytes 1769476
  0.0 4.6 %copy-start.2 = (bf16[256,512]{1,0:T(8,128)(2,1)S(1)}, bf16[256,512]{1,0:T(8,128)(2,1)}, u32[]{:S(2)}) copy-start(bf16[256,512]{1,0:T(8,128)(2,1)} %param.14) | copy-start | bytes 786436
  0.0 5.5 %copy-start.1 = (bf16[256,768]{1,0:T(8,128)(2,1)S(1)}, bf16[256,768]{1,0:T(8,128)(2,1)}, u32[]{:S(2)}) copy-start(bf16[256,768]{1,0:T(8,128)(2,1)} %param.13) | copy-start | bytes 1179652
  0.0 4.6 %copy-start.4 = (f32[512]{0:T(512)S(1)}, f32[512]{0:T(512)}, u32[]{:S(2)}) copy-start(f32[512]{0:T(512)} %param.17) | copy-start | bytes 6148
  0.0 5.4 %copy-start.3 = (f32[768]{0:T(1024)S(1)}, f32[768]{0:T(1024)}, u32[]{:S(2)}) copy-start(f32[768]{0:T(1024)} %param.16) | copy-start | bytes 9220

commit v4 on v3

--- a/solution.py
+++ b/solution.py
@@ -138,7 +138,8 @@
             up_half(me, g),
             {"sp": at_z(k)},
         )
-    send_down(1)
+    for k in range(1, n):
+        send_down(k)
     local = [
         pltpu.make_async_copy(
             up.at[:, pl.ds(pl.multiple_of(me * hid, hid), hid)],
@@ -201,12 +202,14 @@
     norm_all[me, c, x] = normalize(middle[...], gain[...]).astype(jnp.bfloat16)
 
     begin("n", norm_all)
-    for k in range(2, n):
-        send_down(k)
     for k in range(1, n):
         piece = up_half(from_z(k), g)
         land(("up", k), piece)
         send(("uy", k), piece, piece, ypeer)
+    for k in range(1, n):
+        piece = down_half(from_z(k), g)
+        land(("dn", k), piece)
+        send(("dy", k), piece, piece, ypeer)
     finish("n", norm_all)
     for k in range(1, n):
         land(("uy", k), up_half(from_z(k), 1 - g))
@@ -218,10 +221,6 @@
         )
         act[j] = jnp.square(jnp.maximum(upward, 0.0)).astype(jnp.bfloat16)
 
-    for k in range(1, n):
-        piece = down_half(from_z(k), g)
-        land(("dn", k), piece)
-        send(("dy", k), piece, piece, ypeer)
     for k in range(1, n):
         land(("dy", k), down_half(from_z(k), 1 - g))
     local[1].wait()

time: 166 us -> 146 us (0.88)
  Pallas kernels: 156 us -> 136 us
    pallas_call x1, Pallas kernels: 156 us -> 136 us  [run_layer(): pl.pallas_call(lambda *refs: layer_kernel(n, heads, *refs), out_shape=jax...]
where the time goes in v4:
time: 146 us
  Pallas kernels  136 us (93%)
  local copies, waits for them, and re-layouts  5.85 us (4%)
  other arithmetic  3.65 us (2%)
    pallas_call x1, Pallas kernels, run_layer(): pl.pallas_call(lambda *refs: layer_kernel(n, heads, *refs), out_shape=jax...  136 us

profile of v4, /device:TPU:13, one launch (start us, length us, event | category | flops | bytes accessed | tf_op | source)
XLA Modules:
  0.0 145.9 jit_solution(7020414858195453051)
XLA Ops:
  0.0 0.0 copy-start
  0.1 1.2 fusion
  1.3 1.1 fusion.3
  2.4 0.1 multiply_cosine_fusion
  2.6 0.7 fusion.14
  3.3 0.1 copy.44
  3.4 0.1 copy.49
  3.5 0.1 copy.45
  3.6 0.1 copy.50
  3.7 0.8 copy.47
  4.5 0.1 fusion.12
  4.7 0.1 fusion.5
  4.8 0.7 fusion.13.refs_2_
  5.5 0.4 fusion.6
  6.0 0.2 copy.53
  6.2 0.2 copy.46
  6.4 0.2 copy.54
  6.6 0.1 add_convert_fusion
  6.7 0.1 maximum_bitcast_fusion
  6.8 0.8 pad.12.refs_0_
  7.6 0.1 slice.40
  7.7 0.7 pad.13.refs_1_
  8.5 135.8 %shard_map.118 = bf16[64,2048]{1,0:T(8,128)(2,1)} custom-call(bf16[4,256,128]{2,1,0:T(8,128)(2,1)} %pad.12.refs_0_, bf16[4,256,128]{2,1,0:T(8,128)(2,1)} %pad.13.refs_1_, bf16[64,640]{1,0:T(8,128)(2,1)} %fusion.13.refs_2_, bf16[512,512]{1,0:T(8,128)(2,1)} %refs_3_.1, bf16[256,2048]{1,0:T(8,128)(2,1)} %refs_4_.1, bf16[256,2048]{1,0:T(8,128)(2,1)} %refs_5_.1, ...), custom_call_target="tpu_custom_call" | custom-call | tf_op jit(solution)/shard_map/pallas_call | solution.py:284
  144.3 1.7 %copy.56 = bf16[64,2048]{1,0:T(8,128)(2,1)} copy(bf16[64,2048]{1,0:T(8,128)(2,1)} %shard_map.118) | data formatting | bytes 524288
  (19 shorter events, 0.1 us)
Async XLA Ops:
  0.0 5.5 %copy-start = (bf16[768,384]{1,0:T(8,128)(2,1)S(1)}, bf16[768,384]{1,0:T(8,128)(2,1)}, u32[]{:S(2)}) copy-start(bf16[768,384]{1,0:T(8,128)(2,1)} %param.18) | copy-start | bytes 1769476
  0.0 4.6 %copy-start.2 = (bf16[256,512]{1,0:T(8,128)(2,1)S(1)}, bf16[256,512]{1,0:T(8,128)(2,1)}, u32[]{:S(2)}) copy-start(bf16[256,512]{1,0:T(8,128)(2,1)} %param.14) | copy-start | bytes 786436
  0.0 5.5 %copy-start.1 = (bf16[256,768]{1,0:T(8,128)(2,1)S(1)}, bf16[256,768]{1,0:T(8,128)(2,1)}, u32[]{:S(2)}) copy-start(bf16[256,768]{1,0:T(8,128)(2,1)} %param.13) | copy-start | bytes 1179652
  0.0 4.6 %copy-start.4 = (f32[512]{0:T(512)S(1)}, f32[512]{0:T(512)}, u32[]{:S(2)}) copy-start(f32[512]{0:T(512)} %param.17) | copy-start | bytes 6148
  0.0 5.4 %copy-start.3 = (f32[768]{0:T(1024)S(1)}, f32[768]{0:T(1024)}, u32[]{:S(2)}) copy-start(f32[768]{0:T(1024)} %param.16) | copy-start | bytes 9220
